TPU v7x, 32 devices: a whole 2x2x4 slice. The times are simulated.
32 devices in a mesh: rep: 2 (over x), fs: 8 (over z, y), tp: 2 (over core).
Axes of the slice: x: 2, y: 2, z: 4, core: 2. Of those that a mesh axis runs over, the one named last changes fastest.
Arguments:
- mixed_input: bfloat16 [8192, 1024], P(('rep', 'fs', 'tp')), may hold values from -6 to 6
- project_weight: bfloat16 [1024, 1024], P(('fs', 'tp')), may hold values from -0.1875 to 0.1875
- norm_gain: float32 [1024], replicated, may hold values from 0.1 to 1.9
- up_weight: bfloat16 [1024, 4096], P('fs', 'tp'), may hold values from -0.1875 to 0.1875
- down_weight: bfloat16 [4096, 1024], P('tp', 'fs'), may hold values from -0.09375 to 0.09375
Outputs:
- mlp_output: bfloat16 [8192, 1024], P(('rep', 'fs', 'tp'))
All inputs are finite; a program needn't handle non-finite values.
Results may differ from a plain program's by a relative error of at most 0.015.
Values may be sent and summed in bfloat16 or wider, within the bound.
A program may use at most 64 MiB of HBM per device.

v0:
```python
import jax
import jax.numpy as jnp
from jax import lax
from jax.sharding import PartitionSpec as P

epsilon = 1e-06


def gathered_then(section, axis, dim, apply):
    everything = lax.all_gather(section, axis, axis=dim, tiled=True)
    return apply(everything, jnp.int32(0))


def own_rows(contribution, width, axis):
    whole = contribution(jnp.int32(0), width * lax.axis_size(axis)).astype(jnp.bfloat16)
    return lax.psum_scatter(whole, axis, scatter_dimension=0, tiled=True).astype(jnp.float32)


def local(mixed_input, project_weight, norm_gain, up_weight, down_weight):
    whole_project = lax.all_gather(project_weight, ("fs", "tp"), axis=0, tiled=True)
    projected = jnp.dot(mixed_input, whole_project, preferred_element_type=jnp.float32).astype(
        jnp.bfloat16
    )
    values = projected.astype(jnp.float32)
    scale = lax.rsqrt(jnp.mean(values * values, axis=-1, keepdims=True) + epsilon)
    normed = (values * scale * norm_gain.astype(jnp.float32)).astype(jnp.bfloat16)
    up_full = lax.all_gather(up_weight, "fs", axis=0, tiled=True)
    down_full = lax.all_gather(down_weight, "fs", axis=1, tiled=True)

    def lifted(token_piece, first_row):
        preact = jnp.dot(token_piece, up_full, preferred_element_type=jnp.float32)
        return jnp.square(jax.nn.relu(preact)).astype(jnp.bfloat16)

    hidden = gathered_then(normed, "tp", 0, lifted)

    def partial_term(first_row, row_count):
        row_block = lax.dynamic_slice_in_dim(hidden, first_row, row_count, 0)
        return jnp.dot(row_block, down_full, preferred_element_type=jnp.float32)

    summed = own_rows(partial_term, mixed_input.shape[0], "tp")
    return summed.astype(jnp.bfloat16)


def solution(mesh):
    placed = (
        P(("rep", "fs", "tp"), None),
        P(("fs", "tp"), None),
        P(),
        P("fs", "tp"),
        P("tp", "fs"),
    )
    return jax.shard_map(
        local, mesh=mesh, in_specs=placed, out_specs=P(("rep", "fs", "tp"), None), check_vma=False
    )
```

profile of v0, /device:TPU:0, one launch (start us, length us, event | category | flops | bytes accessed | tf_op | source)
XLA Modules:
  0.0 239.4 jit_solution(3866611374542259978)
XLA Ops:
  6.5 0.0 copy-start
  6.5 0.0 all-gather.5.cloned.1.call-start
  6.5 0.7 all-gather.5.cloned.1.call-update
  7.3 0.0 all-gather.7.cloned.1.call-start
  7.3 46.4 %all-gather.5.cloned.1.call-done = bf16[1024,1024]{1,0:T(8,128)(2,1)} async-done(((bf16[64,1024]{1,0:T(8,128)(2,1)}), bf16[1024,1024]{1,0:T(8,128)(2,1)}) %all-gather.5.cloned.1.call-update) | async-done | bytes 2097168 | tf_op jit(solution)/shard_map/all_gather | solution.py:20
  53.7 0.0 copy-done
  53.7 2.4 fusion
  56.1 1.7 fusion.2
  57.8 0.0 all-gather.7.cloned.1.call-update
  57.8 0.0 all-gather.9.cloned.1.call-start
  57.9 0.7 all-gather.9.cloned.1.call-update
  58.5 0.0 all-gather.11.cloned.1.call-start
  58.6 0.5 all-gather.11.cloned.1.call-update
  59.1 0.0 reduce-scatter.2.cloned.1.call-start
  59.2 6.5 %all-gather.7.cloned.1.call-done = bf16[512,1024]{1,0:T(8,128)(2,1)} async-done(((bf16[256,1024]{1,0:T(8,128)(2,1)}), bf16[512,1024]{1,0:T(8,128)(2,1)}) %all-gather.7.cloned.1.call-update) | async-done | bytes 1048592 | tf_op jit(solution)/shard_map/all_gather | solution.py:10
  65.7 76.1 %all-gather.9.cloned.1.call-done = bf16[1024,2048]{1,0:T(8,128)(2,1)} async-done(((bf16[128,2048]{1,0:T(8,128)(2,1)}), bf16[1024,2048]{1,0:T(8,128)(2,1)}) %all-gather.9.cloned.1.call-update) | async-done | bytes 4194320 | tf_op jit(solution)/shard_map/all_gather | solution.py:27
  141.8 75.1 %all-gather.11.cloned.1.call-done = bf16[2048,1024]{1,0:T(8,128)(2,1)} async-done(((bf16[2048,128]{1,0:T(8,128)(2,1)}), bf16[2048,1024]{1,0:T(8,128)(2,1)}) %all-gather.11.cloned.1.call-update) | async-done | bytes 4194320 | tf_op jit(solution)/shard_map/all_gather | solution.py:28
  216.9 9.2 %convolution_convert_fusion = bf16[512,1024]{1,0:T(8,128)(2,1)} fusion(bf16[2048,1024]{1,0:T(8,128)(2,1)} %all-gather.11.cloned.1.call-done, bf16[512,1024]{1,0:T(8,128)(2,1)} %all-gather.7.cloned.1.call-done, bf16[1024,2048]{1,0:T(8,128)(2,1)} %all-gather.9.cloned.1.call-done), kind=kOutput, calls=%fused_computation.1 | convolution fusion | flops 4298637312 | bytes 10485760 | tf_op jit(solution)/shard_map/dot_general | solution.py:38
  226.2 0.0 reduce-scatter.2.cloned.1.call-update
  226.2 6.7 %reduce-scatter.2.cloned.1.call-done = bf16[256,1024]{1,0:T(8,128)(2,1)} async-done(((bf16[512,1024]{1,0:T(8,128)(2,1)}), bf16[256,1024]{1,0:T(8,128)(2,1)}) %reduce-scatter.2.cloned.1.call-update) | async-done | bytes 524304 | tf_op jit(solution)/shard_map/reduce_scatter | solution.py:16
  (1 shorter events, 0.0 us)
Async XLA Ops:
  6.5 47.2 %copy-start = (bf16[256,1024]{1,0:T(8,128)(2,1)S(1)}, bf16[256,1024]{1,0:T(8,128)(2,1)}, u32[]{:S(2)}) copy-start(bf16[256,1024]{1,0:T(8,128)(2,1)} %param.5) | copy-start | bytes 1572868
  6.5 47.2 %all-gather.5.cloned.1.call-start = ((), (), s32[]{:S(2)}) async-start(), calls=%async_computation.1 | async-start | bytes 2228224 | tf_op jit(solution)/shard_map/all_gather | solution.py:20
  7.3 58.4 %all-gather.7.cloned.1.call-start = ((), (), s32[]{:S(2)}) async-start(), calls=%async_computation.2 | async-start | bytes 1572864 | tf_op jit(solution)/shard_map/all_gather | solution.py:10
  57.8 84.0 %all-gather.9.cloned.1.call-start = ((), (), s32[]{:S(2)}) async-start(), calls=%async_computation.3 | async-start | bytes 4718592 | tf_op jit(solution)/shard_map/all_gather | solution.py:27
  58.5 158.4 %all-gather.11.cloned.1.call-start = ((), (), s32[]{:S(2)}) async-start(), calls=%async_computation.4 | async-start | bytes 4718592 | tf_op jit(solution)/shard_map/all_gather | solution.py:28
  59.1 173.8 %reduce-scatter.2.cloned.1.call-start = ((), (), s32[]{:S(2)}) async-start(), calls=%async_computation.5 | async-start | bytes 1572864 | tf_op jit(solution)/shard_map/reduce_scatter | solution.py:16
Sparse Core Ops, SparseCore 0:
  9.5 44.1 all-gather.4
  57.9 7.7 all-gather.6
  67.8 73.9 all-gather.8
  143.7 73.1 all-gather.10
  226.3 6.5 reduce-scatter.1
where the time goes:
time: 240 us; the launch traced here: 239 us
  waiting for transfers between devices  213 us (89%)
  between operations  13.1 us (5%)
  matrix products  11.6 us (5%)
    all_gather x1, waiting for transfers between devices, local(): up_full = lax.all_gather(up_weight, 'fs', axis=0, tiled=True)  76.1 us
    all_gather x1, waiting for transfers between devices, local(): down_full = lax.all_gather(down_weight, 'fs', axis=1, tiled=True)  75.1 us
    all_gather x1, waiting for transfers between devices, local(): lax.all_gather(project_weight, ('fs', 'tp'), axis=0, tiled=True)  46.4 us
    dot_general x1, matrix products, partial_term(): return jnp.dot(row_block, down_full, preferred_element_type=jnp.float32)  9.23 us
    reduce_scatter x1, waiting for transfers between devices, own_rows(): lax.psum_scatter(whole, axis, scatter_dimension=0, tiled=True)  6.73 us
    all_gather x1, waiting for transfers between devices, gathered_then(): everything = lax.all_gather(section, axis, axis=dim, tiled=True)  6.54 us
  transfers between devices with their start and end apart: 5, of which 5 were waited for; matrix products, arithmetic and copies ran while one was open for 0% of the time, Pallas kernels for 0%

commit v1 on v0

--- a/solution.py
+++ b/solution.py
@@ -4,6 +4,11 @@
 from jax.sharding import PartitionSpec as P
 
 epsilon = 1e-06
+
+
+def exchange_gather(array, mesh_axis, dim):
+    stack = jnp.stack([array] * lax.axis_size(mesh_axis))
+    return jnp.concatenate(lax.all_to_all(stack, mesh_axis, 0, 0), axis=dim)
 
 
 def gathered_then(section, axis, dim, apply):
@@ -24,7 +29,7 @@
     values = projected.astype(jnp.float32)
     scale = lax.rsqrt(jnp.mean(values * values, axis=-1, keepdims=True) + epsilon)
     normed = (values * scale * norm_gain.astype(jnp.float32)).astype(jnp.bfloat16)
-    up_full = lax.all_gather(up_weight, "fs", axis=0, tiled=True)
+    up_full = exchange_gather(up_weight, "fs", 0)
     down_full = lax.all_gather(down_weight, "fs", axis=1, tiled=True)
 
     def lifted(token_piece, first_row):

time: 240 us -> 234 us (0.975)
  waiting for transfers between devices: 213 us -> 200 us
  starting transfers between devices: 0.16 us -> 4.69 us
  local copies, waits for them, and re-layouts: 0.01 us -> 2.52 us
    all_to_all x0 -> x1, waiting for transfers between devices: none -> 140 us  [exchange_gather(): return jnp.concatenate(lax.all_to_all(stack, mesh_axis, 0, 0), axis=dim)]
    all_gather x1 -> x0, waiting for transfers between devices: 76.1 us -> none  [local(): up_full = lax.all_gather(up_weight, 'fs', axis=0, tiled=True)]
    all_gather x1, waiting for transfers between devices: 75.1 us -> 4.32 us  [local(): down_full = lax.all_gather(down_weight, 'fs', axis=1, tiled=True)]
    all_gather x1, waiting for transfers between devices: 6.54 us -> 0.02 us  [gathered_then(): everything = lax.all_gather(section, axis, axis=dim, tiled=True)]
    all_to_all x0 -> x1, starting transfers between devices: none -> 4.57 us  [exchange_gather(): return jnp.concatenate(lax.all_to_all(stack, mesh_axis, 0, 0), axis=dim)]
    another operation x0 -> x1, local copies, waits for them, and re-layouts: none -> 2.52 us  [exchange_gather(): stack = jnp.stack([array] * lax.axis_size(mesh_axis))]
  transfers between devices with their start and end apart: 5 -> 5, of which waited for: 5 -> 4; matrix products, arithmetic and copies ran while one was open for 0% -> 1% of each run, Pallas kernels for 0% -> 0%
where the time goes in v1:
time: 234 us
  waiting for transfers between devices  200 us (85%)
  between operations  13.2 us (6%)
  matrix products  11.7 us (5%)
  starting transfers between devices  4.69 us (2%)
  local copies, waits for them, and re-layouts  2.52 us (1%)
    all_to_all x1, waiting for transfers between devices, exchange_gather(): return jnp.concatenate(lax.all_to_all(stack, mesh_axis, 0, 0), axis=dim)  140 us
    all_gather x1, waiting for transfers between devices, local(): lax.all_gather(project_weight, ('fs', 'tp'), axis=0, tiled=True)  46.4 us
    dot_general x1, matrix products, partial_term(): return jnp.dot(row_block, down_full, preferred_element_type=jnp.float32)  9.34 us
    reduce_scatter x1, waiting for transfers between devices, own_rows(): lax.psum_scatter(whole, axis, scatter_dimension=0, tiled=True)  8.44 us
  transfers between devices with their start and end apart: 5, of which 4 were waited for; matrix products, arithmetic and copies ran while one was open for 1% of the time, Pallas kernels for 0%

profile of v1, /device:TPU:0, one launch (start us, length us, event | category | flops | bytes accessed | tf_op | source)
XLA Modules:
  0.0 234.0 jit_solution(1823996413926738483)
XLA Ops:
  6.5 0.0 copy-start
  6.5 0.0 copy-start.1
  6.5 0.0 all-gather.4.cloned.1.call-start
  6.5 0.7 all-gather.4.cloned.1.call-update
  7.3 0.0 all-gather.6.cloned.1.call-start
  7.3 46.4 %all-gather.4.cloned.1.call-done = bf16[1024,1024]{1,0:T(8,128)(2,1)} async-done(((bf16[64,1024]{1,0:T(8,128)(2,1)}), bf16[1024,1024]{1,0:T(8,128)(2,1)}) %all-gather.4.cloned.1.call-update) | async-done | bytes 2097168 | tf_op jit(solution)/shard_map/all_gather | solution.py:25
  53.7 0.0 copy-done
  53.7 2.4 %fusion = (f32[256]{0:T(256)S(1)}, bf16[256,1024]{1,0:T(8,128)(2,1)S(1)}) fusion(bf16[256,1024]{1,0:T(8,128)(2,1)S(1)} %copy-done, bf16[1024,1024]{1,0:T(8,128)(2,1)} %all-gather.4.cloned.1.call-done), kind=kOutput, calls=%fused_computation.5 | convolution fusion | flops 537919232 | bytes 3146752 | tf_op jit(solution)/shard_map/dot_general | solution.py:26
  56.1 1.7 fusion.2
  57.8 0.0 all-gather.6.cloned.1.call-update
  57.8 0.0 copy-done.1
  57.8 2.5 %stack.2 = bf16[8,128,2048]{2,1,0:T(8,128)(2,1)} broadcast(bf16[128,2048]{1,0:T(8,128)(2,1)S(1)} %copy-done.1), dimensions={1,2} | broadcast | bytes 4718592 | tf_op jit(solution)/shard_map/stack | solution.py:10
  60.3 4.6 %all-to-all-start = ((bf16[8,128,2048]{2,1,0:T(8,128)(2,1)}), bf16[8,128,2048]{2,1,0:T(8,128)(2,1)}, u32[]{:S(2)}, u32[]{:S(2)}) async-start(bf16[8,128,2048]{2,1,0:T(8,128)(2,1)} %stack.2), calls=%async_computation | async-start | bytes 8388608 | tf_op jit(solution)/shard_map/all_to_all | solution.py:11
  64.9 0.0 all-gather.8.cloned.1.call-start
  65.0 0.7 all-gather.8.cloned.1.call-update
  65.7 0.0 reduce-scatter.2.cloned.1.call-start
  65.7 0.0 all-gather.6.cloned.1.call-done
  65.7 139.6 %all-to-all-done = bf16[8,128,2048]{2,1,0:T(8,128)(2,1)} async-done(((bf16[8,128,2048]{2,1,0:T(8,128)(2,1)}), bf16[8,128,2048]{2,1,0:T(8,128)(2,1)}, u32[]{:S(2)}, u32[]{:S(2)}) %all-to-all-start) | async-done | bytes 4194336 | tf_op jit(solution)/shard_map/all_to_all | solution.py:11
  205.3 4.3 %all-gather.8.cloned.1.call-done = bf16[2048,1024]{1,0:T(8,128)(2,1)} async-done(((bf16[2048,128]{1,0:T(8,128)(2,1)}), bf16[2048,1024]{1,0:T(8,128)(2,1)}) %all-gather.8.cloned.1.call-update) | async-done | bytes 4194320 | tf_op jit(solution)/shard_map/all_gather | solution.py:33
  209.6 9.3 %convolution_convert_fusion = bf16[512,1024]{1,0:T(8,128)(2,1)} fusion(bf16[2048,1024]{1,0:T(8,128)(2,1)} %all-gather.8.cloned.1.call-done, bf16[512,1024]{1,0:T(8,128)(2,1)} %all-gather.6.cloned.1.call-done, bf16[1024,2048]{1,0:T(8,128)(2,1)} %bitcast), kind=kOutput, calls=%fused_computation.1 | convolution fusion | flops 4298637312 | bytes 10485760 | tf_op jit(solution)/shard_map/dot_general | solution.py:43
  219.0 0.0 reduce-scatter.2.cloned.1.call-update
  219.0 8.4 %reduce-scatter.2.cloned.1.call-done = bf16[256,1024]{1,0:T(8,128)(2,1)} async-done(((bf16[512,1024]{1,0:T(8,128)(2,1)}), bf16[256,1024]{1,0:T(8,128)(2,1)}) %reduce-scatter.2.cloned.1.call-update) | async-done | bytes 524304 | tf_op jit(solution)/shard_map/reduce_scatter | solution.py:21
  (1 shorter events, 0.0 us)
Async XLA Ops:
  6.5 47.2 %copy-start = (bf16[256,1024]{1,0:T(8,128)(2,1)S(1)}, bf16[256,1024]{1,0:T(8,128)(2,1)}, u32[]{:S(2)}) copy-start(bf16[256,1024]{1,0:T(8,128)(2,1)} %param.5) | copy-start | bytes 1572868
  6.5 51.3 %copy-start.1 = (bf16[128,2048]{1,0:T(8,128)(2,1)S(1)}, bf16[128,2048]{1,0:T(8,128)(2,1)}, u32[]{:S(2)}) copy-start(bf16[128,2048]{1,0:T(8,128)(2,1)} %param.8) | copy-start | bytes 1572868
  6.5 47.2 %all-gather.4.cloned.1.call-start = ((), (), s32[]{:S(2)}) async-start(), calls=%async_computation.2 | async-start | bytes 2228224 | tf_op jit(solution)/shard_map/all_gather | solution.py:25
  7.3 58.5 %all-gather.6.cloned.1.call-start = ((), (), s32[]{:S(2)}) async-start(), calls=%async_computation.3 | async-start | bytes 1572864 | tf_op jit(solution)/shard_map/all_gather | solution.py:15
  60.3 145.0 %all-to-all-start = ((bf16[8,128,2048]{2,1,0:T(8,128)(2,1)}), bf16[8,128,2048]{2,1,0:T(8,128)(2,1)}, u32[]{:S(2)}, u32[]{:S(2)}) async-start(bf16[8,128,2048]{2,1,0:T(8,128)(2,1)} %stack.2), calls=%async_computation | async-start | bytes 8388608 | tf_op jit(solution)/shard_map/all_to_all | solution.py:11
  64.9 144.7 %all-gather.8.cloned.1.call-start = ((), (), s32[]{:S(2)}) async-start(), calls=%async_computation.4 | async-start | bytes 4718592 | tf_op jit(solution)/shard_map/all_gather | solution.py:33
  65.7 161.8 %reduce-scatter.2.cloned.1.call-start = ((), (), s32[]{:S(2)}) async-start(), calls=%async_computation.5 | async-start | bytes 1572864 | tf_op jit(solution)/shard_map/reduce_scatter | solution.py:21
Sparse Core Ops, SparseCore 0:
  9.5 44.1 all-gather.3
  57.9 7.7 all-gather.5
  67.8 141.8 all-gather.7
  219.1 8.2 reduce-scatter.1
